TPU v7x, 32 devices: a whole 2x2x4 slice. The times are simulated.
32 devices in a mesh: ep: 8 (over z, x), tp: 4 (over y, core).
Axes of the slice: x: 2, y: 2, z: 4, core: 2. Of those that a mesh axis runs over, the one named last changes fastest.
Arguments:
- tokens: bfloat16 [512, 4096], P('ep'), may hold values from -6 to 6
- state_in: float32 [512, 4096], P('ep', 'tp'), may hold values from -6 to 6
- conv_in: bfloat16 [512, 3, 4096], P('ep', None, 'tp'), may hold values from -6 to 6
- mix_gain: bfloat16 [4096], replicated, may hold values from 0.099609375 to 1.8984375
- rnn_weight: bfloat16 [4096, 4096], P('ep', 'tp'), may hold values from -0.09375 to 0.09375
- gate_weight: bfloat16 [4096, 4096], P('ep', 'tp'), may hold values from -0.09375 to 0.09375
- conv_weight: bfloat16 [4, 4096], P(None, 'tp'), may hold values from -3 to 3
- rate_weight: bfloat16 [16, 256, 256], P('tp'), may hold values from -0.375 to 0.375
- input_weight: bfloat16 [16, 256, 256], P('tp'), may hold values from -0.375 to 0.375
- rate_param: float32 [4096], P('tp'), may hold values from 1 to 6
- out_weight: bfloat16 [4096, 4096], P('tp'), may hold values from -0.09375 to 0.09375
- moe_gain: bfloat16 [4096], replicated, may hold values from 0.099609375 to 1.8984375
- expert_gate: bfloat16 [8, 4096, 2048], P('ep', None, 'tp'), may hold values from -0.09375 to 0.09375
- expert_up: bfloat16 [8, 4096, 2048], P('ep', None, 'tp'), may hold values from -0.09375 to 0.09375
- expert_down: bfloat16 [8, 2048, 4096], P('ep', 'tp'), may hold values from -0.125 to 0.125
- routes: int32 [512, 2], P('ep'), may hold values from 0 to 7, all different within a row; in each aligned block of 64 rows (0 to 63, 64 to 127, ...) at most 32 rows name the same one
- route_prob: float32 [512, 2], P('ep'), may hold values from 0.1 to 1
Outputs:
- layer_out: bfloat16 [512, 4096], P('ep', 'tp')
- state_out: float32 [512, 4096], P('ep', 'tp')
- conv_out: bfloat16 [512, 3, 4096], P('ep', None, 'tp')
Inputs may be any that keep to these rules, and one draw needn't show every extreme that they name: `routes`: the 2 experts of a sequence differ. Among the rows of one index of ep no expert is named more than 32 times, and in every draw some expert is named exactly 32 times there.
All inputs are finite; a program needn't handle non-finite values.
Results may differ from a plain program's by a relative error of at most 0.014.
Values may be sent and summed in bfloat16 or wider, within the bound.
A program may use at most 64 MiB of HBM per device.

v0:
```python
import jax
import jax.numpy as jnp
from jax import lax
from jax.sharding import PartitionSpec as P


def rms_scale(values, gain):
    scale = lax.rsqrt(jnp.mean(values * values, axis=-1, keepdims=True) + 1e-06)
    return values * scale * gain.astype(jnp.float32)


def slot_targets(route_ids, experts, capacity):
    flat_ids = route_ids.reshape(-1)
    onehot = (flat_ids[:, None] == jnp.arange(experts, dtype=jnp.int32)[None, :]).astype(jnp.int32)
    before = jnp.cumsum(onehot, axis=0) - onehot
    slot_ids = jnp.sum(before * onehot, axis=1)
    return flat_ids * capacity + slot_ids


def block_map(conv, weight):
    rows = conv.shape[0]
    blocks = weight.shape[0]
    parts = conv.reshape(rows, blocks, weight.shape[1])
    mapped = jnp.einsum("snc,ncd->snd", parts, weight, preferred_element_type=jnp.float32)
    return mapped.reshape(rows, blocks * weight.shape[2])


def shards(
    tokens,
    state_in,
    conv_in,
    mix_gain,
    rnn_weight,
    gate_weight,
    conv_weight,
    rate_weight,
    input_weight,
    rate_param,
    out_weight,
    moe_gain,
    expert_gate,
    expert_up,
    expert_down,
    routes,
    route_prob,
):
    group_rows = tokens.shape[0]
    model_width = tokens.shape[1]
    channels = rnn_weight.shape[1]
    base = tokens.astype(jnp.float32)
    normed = rms_scale(base, mix_gain).astype(jnp.bfloat16)
    columns = lax.all_to_all(normed, "ep", split_axis=1, concat_axis=0, tiled=True)
    joined = jnp.concatenate([rnn_weight, gate_weight], axis=1)
    summed = lax.psum_scatter(
        jnp.dot(columns, joined, preferred_element_type=jnp.float32).astype(jnp.bfloat16),
        "ep",
        scatter_dimension=0,
        tiled=True,
    ).astype(jnp.float32)
    proj_x = summed[:, :channels]
    proj_y = summed[:, channels:]
    moved = proj_x.astype(jnp.bfloat16)
    conv_out = jnp.concatenate([conv_in[:, 1:], moved[:, None, :]], axis=1)
    taps = conv_weight.astype(jnp.float32)
    history = conv_in.astype(jnp.float32)
    mixed_in = (
        history[:, 0] * taps[0]
        + history[:, 1] * taps[1]
        + history[:, 2] * taps[2]
        + moved.astype(jnp.float32) * taps[3]
    )
    conv = mixed_in.astype(jnp.bfloat16)
    rate = jax.nn.sigmoid(block_map(conv, rate_weight))
    in_gate = jax.nn.sigmoid(block_map(conv, input_weight))
    log_decay = -8.0 * rate * jax.nn.softplus(-rate_param)
    state_out = jnp.exp(log_decay) * state_in + jnp.sqrt(
        -jnp.expm1(2.0 * log_decay)
    ) * in_gate * conv.astype(jnp.float32)
    gated = (state_out * jax.nn.gelu(proj_y, approximate=True)).astype(jnp.bfloat16)
    partial_out = jnp.dot(gated, out_weight, preferred_element_type=jnp.float32)
    mixed = base + lax.psum(partial_out.astype(jnp.bfloat16), "tp").astype(jnp.float32)
    normed2 = rms_scale(mixed, moe_gain).astype(jnp.bfloat16)
    experts = lax.axis_size("ep")
    topk = routes.shape[1]
    capacity = max(2, 2 * group_rows * topk // experts)
    targets = slot_targets(routes, experts, capacity)
    dispatch = (
        jnp.arange(experts * capacity, dtype=jnp.int32)[:, None] == targets[None, :]
    ).astype(jnp.bfloat16)
    repeated = jnp.repeat(normed2, topk, axis=0)
    send = jnp.dot(dispatch, repeated, preferred_element_type=jnp.float32).astype(jnp.bfloat16)
    send = send.reshape(experts, capacity, model_width)
    received = lax.all_to_all(send, "ep", split_axis=0, concat_axis=0, tiled=True)
    flat_rows = received.reshape(-1, model_width)
    gate_part = jnp.dot(flat_rows, expert_gate[0], preferred_element_type=jnp.float32)
    up_part = jnp.dot(flat_rows, expert_up[0], preferred_element_type=jnp.float32)
    hidden = (jax.nn.silu(gate_part) * up_part).astype(jnp.bfloat16)
    result = jnp.dot(hidden, expert_down[0], preferred_element_type=jnp.float32)
    partial_experts = result.reshape(received.shape[0], received.shape[1], model_width)
    reduced = lax.psum_scatter(
        partial_experts.astype(jnp.bfloat16), "tp", scatter_dimension=2, tiled=True
    )
    returned = lax.all_to_all(reduced, "ep", split_axis=0, concat_axis=0, tiled=True)
    share = returned.shape[2]
    picked = jnp.einsum(
        "rj,rd->jd",
        dispatch,
        returned.reshape(experts * capacity, share),
        preferred_element_type=jnp.float32,
    )
    weights = route_prob / jnp.sum(route_prob, axis=1, keepdims=True)
    experts_sum = jnp.sum(picked.reshape(group_rows, topk, share) * weights[:, :, None], axis=1)
    own_columns = lax.dynamic_slice_in_dim(mixed, lax.axis_index("tp") * share, share, 1)
    layer_out = (own_columns + experts_sum).astype(jnp.bfloat16)
    return (layer_out, state_out, conv_out)


def solution(mesh):
    in_specs = (
        P("ep", None),
        P("ep", "tp"),
        P("ep", None, "tp"),
        P(),
        P("ep", "tp"),
        P("ep", "tp"),
        P(None, "tp"),
        P("tp", None, None),
        P("tp", None, None),
        P("tp"),
        P("tp", None),
        P(),
        P("ep", None, "tp"),
        P("ep", None, "tp"),
        P("ep", "tp", None),
        P("ep", None),
        P("ep", None),
    )
    out_specs = (P("ep", "tp"), P("ep", "tp"), P("ep", None, "tp"))
    return jax.shard_map(shards, mesh=mesh, in_specs=in_specs, out_specs=out_specs, check_vma=False)
```

profile of v0, /device:TPU:0, one launch (start us, length us, event | category | flops | bytes accessed | tf_op | source)
XLA Modules:
  0.0 267.9 jit_solution(9502218566155616131)
XLA Ops:
  7.2 0.7 convert_element_type.63
  8.0 1.2 fusion.23
  9.2 1.2 fusion.25
  10.5 21.6 %all_to_all.29 = bf16[64,8,512]{2,0,1:T(8,128)(2,1)S(1)} all-to-all(bf16[64,8,512]{2,0,1:T(8,128)(2,1)S(1)} %bitcast.85), channel_id=1, replica_groups=mesh['ep'=8,'tp'=4] {'ep'}, dimensions={1} | all-to-all | bytes 1048576 | tf_op jit(solution)/shard_map/all_to_all | solution.py:52
  32.1 4.2 %convolution_convert_fusion.3 = bf16[512,2048]{1,0:T(8,128)(2,1)} fusion(bf16[512,512]{1,0:T(8,128)(2,1)S(1)} %bitcast.88, bf16[512,1024]{1,0:T(8,128)(2,1)} %param.22, bf16[512,1024]{1,0:T(8,128)(2,1)} %param.21), kind=kOutput, calls=%fused_computation.8 | convolution fusion | flops 1078984704 | bytes 4718592 | tf_op jit(solution)/shard_map/dot_general | solution.py:55
  36.6 0.1 reshape.101
  36.8 0.2 reduce_window_sum.11
  37.1 66.8 %reduce-scatter.3.cloned.1.call-done = bf16[64,2048]{1,0:T(8,128)(2,1)} async-done(((bf16[512,2048]{1,0:T(8,128)(2,1)}), bf16[64,2048]{1,0:T(8,128)(2,1)}) %reduce-scatter.3.cloned.1.call-update) | async-done | bytes 262160 | tf_op jit(solution)/shard_map/reduce_scatter | solution.py:54
  103.8 1.1 fusion.36
  104.9 0.2 fusion.22
  105.2 0.2 fusion.18
  105.5 0.2 multiply_add_fusion
  105.8 5.9 %convolution_convert_fusion.2 = bf16[64,4096]{1,0:T(8,128)(2,1)} fusion(bf16[1024,4096]{1,0:T(8,128)(2,1)} %param.27, f32[64,1024]{1,0:T(8,128)S(1)} %multiply_add_fusion, bf16[64,2048]{1,0:T(8,128)(2,1)S(1)} %copy-done.4), kind=kOutput, calls=%fused_computation.2 | convolution fusion | flops 537853952 | bytes 9306112 | tf_op jit(solution)/shard_map/dot_general | solution.py:80
  111.7 0.2 select_reduce_fusion
  111.9 32.4 %all-reduce.2.cloned.1.call-done = bf16[64,4096]{1,0:T(8,128)(2,1)} async-done(((bf16[64,4096]{1,0:T(8,128)(2,1)}), bf16[64,4096]{1,0:T(8,128)(2,1)}) %all-reduce.2.cloned.1.call-update) | async-done | bytes 524304 | tf_op jit(solution)/shard_map/psum | solution.py:81
  144.3 2.3 convert_add_fusion
  146.6 1.3 multiply_convert_fusion
  147.9 1.0 broadcast_in_dim.4
  148.9 0.4 reshape.102
  149.4 0.7 convolution_convert_fusion
  150.1 52.8 %all_to_all.30 = bf16[8,32,4096]{2,1,0:T(8,128)(2,1)S(1)} all-to-all(bf16[8,32,4096]{2,1,0:T(8,128)(2,1)S(1)} %bitcast.80), channel_id=1, replica_groups=mesh['ep'=8,'tp'=4] {'ep'}, dimensions={0} | all-to-all | bytes 4194304 | tf_op jit(solution)/shard_map/all_to_all | solution.py:93
  202.9 1.2 fusion.3
  204.1 0.9 copy-done.12
  205.1 1.3 fusion.11
  206.3 0.9 copy-done.13
  207.2 2.6 convolution_convert_fusion.1
  209.9 29.8 %reduce-scatter.5.cloned.1.call-done = bf16[8,32,1024]{2,1,0:T(8,128)(2,1)} async-done(((bf16[8,32,4096]{2,1,0:T(8,128)(2,1)}), bf16[8,32,1024]{2,1,0:T(8,128)(2,1)}) %reduce-scatter.5.cloned.1.call-update) | async-done | bytes 524304 | tf_op jit(solution)/shard_map/reduce_scatter | solution.py:100
  239.7 5.5 %all-to-all-start.2 = ((bf16[8,32,1024]{2,1,0:T(8,128)(2,1)}), bf16[8,32,1024]{2,1,0:T(8,128)(2,1)S(1)}, u32[]{:S(2)}, u32[]{:S(2)}) async-start(bf16[8,32,1024]{2,1,0:T(8,128)(2,1)} %reduce-scatter.5.cloned.1.call-done), calls=%async_computation.4 | async-start | bytes 1048576 | tf_op jit(solution)/shard_map/all_to_all | solution.py:103
  245.4 0.8 pad_maximum_fusion
  246.2 13.3 %all-to-all-done.2 = bf16[8,32,1024]{2,1,0:T(8,128)(2,1)S(1)} async-done(((bf16[8,32,1024]{2,1,0:T(8,128)(2,1)}), bf16[8,32,1024]{2,1,0:T(8,128)(2,1)S(1)}, u32[]{:S(2)}, u32[]{:S(2)}) %all-to-all-start.2) | async-done | bytes 524320 | tf_op jit(solution)/shard_map/all_to_all | solution.py:103
  259.5 0.2 fusion.14
  259.7 1.6 add_convert_fusion
  (53 shorter events, 0.8 us)
Async XLA Ops:
  7.2 97.7 %copy-start = (bf16[4,256,256]{2,1,0:T(8,128)(2,1)S(1)}, bf16[4,256,256]{2,1,0:T(8,128)(2,1)}, u32[]{:S(2)}) copy-start(bf16[4,256,256]{2,1,0:T(8,128)(2,1)} %param.24) | copy-start | bytes 1572868
  7.2 96.7 %reduce-scatter.3.cloned.1.call-start = ((), (), s32[]{:S(2)}) async-start(), calls=%async_computation.5 | async-start | bytes 2359296 | tf_op jit(solution)/shard_map/reduce_scatter | solution.py:54
  32.1 4.3 %copy-start.3 = (bf16[64,3,1024]{2,0,1:T(8,128)(2,1)S(1)}, bf16[64,3,1024]{2,0,1:T(8,128)(2,1)}, u32[]{:S(2)}) copy-start(bf16[64,3,1024]{2,0,1:T(8,128)(2,1)} %param.19) | copy-start | bytes 1179652
  32.1 4.4 %copy-start.10 = (s32[64,2]{0,1:T(2,128)S(1)}, s32[64,2]{0,1:T(2,128)}, u32[]{:S(2)}) copy-start(s32[64,2]{0,1:T(2,128)} %param.32) | copy-start | bytes 1540
  32.1 4.9 %copy-start.8 = (f32[1024]{0:T(1024)S(1)}, f32[1024]{0:T(1024)}, u32[]{:S(2)}) copy-start(f32[1024]{0:T(1024)} %param.26) | copy-start | bytes 12292
  32.1 4.9 %copy-start.6 = (bf16[4,1024]{1,0:T(4,128)(2,1)S(1)}, bf16[4,1024]{1,0:T(4,128)(2,1)}, u32[]{:S(2)}) copy-start(bf16[4,1024]{1,0:T(4,128)(2,1)} %param.23) | copy-start | bytes 24580
  36.3 68.9 %copy-start.14 = (bf16[4,256,256]{2,1,0:T(8,128)(2,1)S(1)}, bf16[4,256,256]{2,1,0:T(8,128)(2,1)}, u32[]{:S(2)}) copy-start(bf16[4,256,256]{2,1,0:T(8,128)(2,1)} %param.25) | copy-start | bytes 1572868
  36.3 69.2 %copy-start.5 = (f32[64,1024]{1,0:T(8,128)S(1)}, f32[64,1024]{1,0:T(8,128)}, u32[]{:S(2)}) copy-start(f32[64,1024]{1,0:T(8,128)} %param.18) | copy-start | bytes 786436
  36.4 107.9 %all-reduce.2.cloned.1.call-start = ((), (), s32[]{:S(2)}) async-start(), calls=%async_computation.6 | async-start | bytes 1048576 | tf_op jit(solution)/shard_map/psum | solution.py:81
  103.8 1.9 copy-start.4
  105.7 5.9 %copy-start.2 = (f32[64,1024]{1,0:T(8,128)}, f32[64,1024]{1,0:T(8,128)S(1)}, u32[]{:S(2)}) copy-start(f32[64,1024]{1,0:T(8,128)S(1)} %multiply_add_fusion) | copy-start | bytes 786436
  105.7 6.2 %copy-start.7 = (bf16[4096]{0:T(1024)(128)(2,1)S(1)}, bf16[4096]{0:T(1024)(128)(2,1)}, u32[]{:S(2)}) copy-start(bf16[4096]{0:T(1024)(128)(2,1)} %param.28) | copy-start | bytes 24580
  105.8 38.5 %copy-start.1 = (bf16[64,4096]{1,0:T(8,128)(2,1)S(1)}, bf16[64,4096]{1,0:T(8,128)(2,1)}, u32[]{:S(2)}) copy-start(bf16[64,4096]{1,0:T(8,128)(2,1)} %param.17) | copy-start | bytes 1572868
  111.7 128.0 %reduce-scatter.5.cloned.1.call-start = ((), (), s32[]{:S(2)}) async-start(), calls=%async_computation.7 | async-start | bytes 2621440 | tf_op jit(solution)/shard_map/reduce_scatter | solution.py:100
  149.3 53.5 %copy-start.11 = (bf16[1,4096,512]{2,1,0:T(8,128)(2,1)S(1)}, bf16[1,4096,512]{2,1,0:T(8,128)(2,1)}, u32[]{:S(2)}) copy-start(bf16[1,4096,512]{2,1,0:T(8,128)(2,1)} %param.29) | copy-start | bytes 12582916
  202.9 2.2 copy-start.12
  205.1 2.2 copy-start.13
  207.2 38.1 %copy-start.9 = (f32[64,2]{0,1:T(2,128)S(1)}, f32[64,2]{0,1:T(2,128)}, u32[]{:S(2)}) copy-start(f32[64,2]{0,1:T(2,128)} %param.33) | copy-start | bytes 1540
  207.2 38.1 %slice-start = ((bf16[64,3,1024]{2,0,1:T(8,128)(2,1)}), bf16[64,2,1024]{2,0,1:T(8,128)(2,1)S(1)}, s32[]{:S(2)}) async-start(bf16[64,3,1024]{2,0,1:T(8,128)(2,1)} %param.19), calls=%async_computation.8 | async-start | bytes 524288 | tf_op jit(solution)/shard_map/slice | solution.py:63
  239.7 19.8 %all-to-all-start.2 = ((bf16[8,32,1024]{2,1,0:T(8,128)(2,1)}), bf16[8,32,1024]{2,1,0:T(8,128)(2,1)S(1)}, u32[]{:S(2)}, u32[]{:S(2)}) async-start(bf16[8,32,1024]{2,1,0:T(8,128)(2,1)} %reduce-scatter.5.cloned.1.call-done), calls=%async_computation.4 | async-start | bytes 1048576 | tf_op jit(solution)/shard_map/all_to_all | solution.py:103
Sparse Core Ops, SparseCore 0:
  36.5 67.3 reduce-scatter.2
  111.8 32.4 all-reduce.1
  210.0 29.6 reduce-scatter.4
where the time goes:
time: 269 us; the launch traced here: 268 us
  waiting for transfers between devices  142 us (53%)
  blocking collectives  74.4 us (28%)
  matrix products  16.6 us (6%)
  between operations  14.1 us (5%)
  other arithmetic  11.2 us (4%)
  starting transfers between devices  5.64 us (2%)
  local copies, waits for them, and re-layouts  3.75 us (1%)
    reduce_scatter x1, waiting for transfers between devices, shards(): lax.psum_scatter(jnp.dot(columns, joined, preferred_element_type=jnp.floa...  66.8 us
    all_to_all x1, blocking collectives, shards(): lax.all_to_all(send, 'ep', split_axis=0, concat_axis=0, tiled=True)  52.8 us
    psum x1, waiting for transfers between devices, shards(): lax.psum(partial_out.astype(jnp.bfloat16), 'tp').astype(jnp.float32)  32.4 us
    reduce_scatter x1, waiting for transfers between devices, shards(): lax.psum_scatter(partial_experts.astype(jnp.bfloat16), 'tp', scatter_dime...  29.8 us
    all_to_all x1, blocking collectives, shards(): lax.all_to_all(normed, 'ep', split_axis=1, concat_axis=0, tiled=True)  21.6 us
    all_to_all x1, waiting for transfers between devices, shards(): lax.all_to_all(reduced, 'ep', split_axis=0, concat_axis=0, tiled=True)  13.3 us
    dot_general x1, matrix products, shards(): partial_out = jnp.dot(gated, out_weight, preferred_element_type=jnp.float32)  5.88 us
    all_to_all x1, starting transfers between devices, shards(): lax.all_to_all(reduced, 'ep', split_axis=0, concat_axis=0, tiled=True)  5.51 us
  transfers between devices with their start and end apart: 4, of which 4 were waited for; matrix products, arithmetic and copies ran while one was open for 1% of the time, Pallas kernels for 0%

commit v1 on v0

--- a/solution.py
+++ b/solution.py
@@ -78,7 +78,9 @@
     ) * in_gate * conv.astype(jnp.float32)
     gated = (state_out * jax.nn.gelu(proj_y, approximate=True)).astype(jnp.bfloat16)
     partial_out = jnp.dot(gated, out_weight, preferred_element_type=jnp.float32)
-    mixed = base + lax.psum(partial_out.astype(jnp.bfloat16), "tp").astype(jnp.float32)
+    mixed = base + jnp.sum(lax.all_gather(partial_out.astype(jnp.bfloat16), "tp"), axis=0).astype(
+        jnp.float32
+    )
     normed2 = rms_scale(mixed, moe_gain).astype(jnp.bfloat16)
     experts = lax.axis_size("ep")
     topk = routes.shape[1]

time: 269 us -> 259 us (0.963)
  waiting for transfers between devices: 142 us -> 131 us
    psum x1 -> x0, waiting for transfers between devices: 32.4 us -> none  [shards(): lax.psum(partial_out.astype(jnp.bfloat16), 'tp').astype(jnp.float32)]
    all_gather x0 -> x1, waiting for transfers between devices: none -> 21 us  [shards(): lax.all_gather(partial_out.astype(jnp.bfloat16), 'tp')]
where the time goes in v1:
time: 259 us; the launch traced here: 258 us
  waiting for transfers between devices  131 us (51%)
  blocking collectives  75.6 us (29%)
  matrix products  16.6 us (6%)
  between operations  14.1 us (5%)
  other arithmetic  11.1 us (4%)
  starting transfers between devices  5.63 us (2%)
  local copies, waits for them, and re-layouts  3.76 us (1%)
    reduce_scatter x1, waiting for transfers between devices, shards(): lax.psum_scatter(jnp.dot(columns, joined, preferred_element_type=jnp.floa...  67.6 us
    all_to_all x1, blocking collectives, shards(): lax.all_to_all(send, 'ep', split_axis=0, concat_axis=0, tiled=True)  54 us
    reduce_scatter x1, waiting for transfers between devices, shards(): lax.psum_scatter(partial_experts.astype(jnp.bfloat16), 'tp', scatter_dime...  29.4 us
    all_to_all x1, blocking collectives, shards(): lax.all_to_all(normed, 'ep', split_axis=1, concat_axis=0, tiled=True)  21.6 us
    all_gather x1, waiting for transfers between devices, shards(): lax.all_gather(partial_out.astype(jnp.bfloat16), 'tp')  21 us
    all_to_all x1, waiting for transfers between devices, shards(): lax.all_to_all(reduced, 'ep', split_axis=0, concat_axis=0, tiled=True)  13.3 us
    dot_general x1, matrix products, shards(): partial_out = jnp.dot(gated, out_weight, preferred_element_type=jnp.float32)  5.89 us
    all_to_all x1, starting transfers between devices, shards(): lax.all_to_all(reduced, 'ep', split_axis=0, concat_axis=0, tiled=True)  5.51 us
  transfers between devices with their start and end apart: 4, of which 4 were waited for; matrix products, arithmetic and copies ran while one was open for 1% of the time, Pallas kernels for 0%

profile of v1, /device:TPU:0, one launch (start us, length us, event | category | flops | bytes accessed | tf_op | source)
XLA Modules:
  0.0 258.2 jit_solution(1924635877569639972)
XLA Ops:
  7.2 0.7 convert_element_type.65
  8.0 1.2 fusion.23
  9.2 1.2 fusion.25
  10.5 21.6 %all_to_all.29 = bf16[64,8,512]{2,0,1:T(8,128)(2,1)S(1)} all-to-all(bf16[64,8,512]{2,0,1:T(8,128)(2,1)S(1)} %bitcast.87), channel_id=1, replica_groups=mesh['ep'=8,'tp'=4] {'ep'}, dimensions={1} | all-to-all | bytes 1048576 | tf_op jit(solution)/shard_map/all_to_all | solution.py:52
  32.1 4.2 %convolution_convert_fusion.3 = bf16[512,2048]{1,0:T(8,128)(2,1)} fusion(bf16[512,512]{1,0:T(8,128)(2,1)S(1)} %bitcast.90, bf16[512,1024]{1,0:T(8,128)(2,1)} %param.22, bf16[512,1024]{1,0:T(8,128)(2,1)} %param.21), kind=kOutput, calls=%fused_computation.8 | convolution fusion | flops 1078984704 | bytes 4718592 | tf_op jit(solution)/shard_map/dot_general | solution.py:55
  36.5 67.6 %reduce-scatter.3.cloned.1.call-done = bf16[64,2048]{1,0:T(8,128)(2,1)} async-done(((bf16[512,2048]{1,0:T(8,128)(2,1)}), bf16[64,2048]{1,0:T(8,128)(2,1)}) %reduce-scatter.3.cloned.1.call-update) | async-done | bytes 262160 | tf_op jit(solution)/shard_map/reduce_scatter | solution.py:54
  104.1 1.1 fusion.36
  105.2 0.2 fusion.22
  105.5 0.2 fusion.18
  105.8 0.2 multiply_add_fusion
  106.1 5.9 %convolution_convert_fusion.2 = bf16[64,4096]{1,0:T(8,128)(2,1)} fusion(bf16[1024,4096]{1,0:T(8,128)(2,1)} %param.27, f32[64,1024]{1,0:T(8,128)S(1)} %multiply_add_fusion, bf16[64,2048]{1,0:T(8,128)(2,1)S(1)} %copy-done.4), kind=kOutput, calls=%fused_computation.2 | convolution fusion | flops 537853952 | bytes 9306112 | tf_op jit(solution)/shard_map/dot_general | solution.py:80
  112.4 0.2 reduce_window_sum.11
  112.6 0.2 select_reduce_fusion
  112.8 21.0 %all-gather.3.cloned.1.call-done = bf16[256,4096]{1,0:T(8,128)(2,1)} async-done(((bf16[64,4096]{1,0:T(8,128)(2,1)}), bf16[256,4096]{1,0:T(8,128)(2,1)}) %all-gather.3.cloned.1.call-update) | async-done | bytes 2097168 | tf_op jit(solution)/shard_map/all_gather | solution.py:81
  133.8 2.0 reduce_sum.58
  135.8 1.3 convert_add_fusion
  137.1 0.2 multiply_convert_fusion
  137.3 1.0 broadcast_in_dim.4
  138.3 0.4 reshape.102
  138.8 0.7 convolution_convert_fusion
  139.5 54.0 %all_to_all.30 = bf16[8,32,4096]{2,1,0:T(8,128)(2,1)S(1)} all-to-all(bf16[8,32,4096]{2,1,0:T(8,128)(2,1)S(1)} %bitcast.81), channel_id=1, replica_groups=mesh['ep'=8,'tp'=4] {'ep'}, dimensions={0} | all-to-all | bytes 4194304 | tf_op jit(solution)/shard_map/all_to_all | solution.py:95
  193.5 1.2 fusion.3
  194.7 0.9 copy-done.12
  195.7 1.3 fusion.11
  196.9 0.9 copy-done.13
  197.9 2.6 %convolution_convert_fusion.1 = bf16[8,32,4096]{2,1,0:T(8,128)(2,1)} fusion(bf16[8,32,512]{2,1,0:T(8,128)(2,1)S(1)} %bitcast.97, bf16[1,512,4096]{2,1,0:T(8,128)(2,1)S(1)} %copy-done.13), kind=kOutput, calls=%fused_computation.1 | convolution fusion | flops 1074790400 | bytes 6553600 | tf_op jit(solution)/shard_map/dot_general | solution.py:100
  200.5 29.4 %reduce-scatter.5.cloned.1.call-done = bf16[8,32,1024]{2,1,0:T(8,128)(2,1)} async-done(((bf16[8,32,4096]{2,1,0:T(8,128)(2,1)}), bf16[8,32,1024]{2,1,0:T(8,128)(2,1)}) %reduce-scatter.5.cloned.1.call-update) | async-done | bytes 524304 | tf_op jit(solution)/shard_map/reduce_scatter | solution.py:102
  229.9 5.5 %all-to-all-start.2 = ((bf16[8,32,1024]{2,1,0:T(8,128)(2,1)}), bf16[8,32,1024]{2,1,0:T(8,128)(2,1)S(1)}, u32[]{:S(2)}, u32[]{:S(2)}) async-start(bf16[8,32,1024]{2,1,0:T(8,128)(2,1)} %reduce-scatter.5.cloned.1.call-done), calls=%async_computation.4 | async-start | bytes 1048576 | tf_op jit(solution)/shard_map/all_to_all | solution.py:105
  235.6 0.8 pad_maximum_fusion
  236.4 13.3 %all-to-all-done.2 = bf16[8,32,1024]{2,1,0:T(8,128)(2,1)S(1)} async-done(((bf16[8,32,1024]{2,1,0:T(8,128)(2,1)}), bf16[8,32,1024]{2,1,0:T(8,128)(2,1)S(1)}, u32[]{:S(2)}, u32[]{:S(2)}) %all-to-all-start.2) | async-done | bytes 524320 | tf_op jit(solution)/shard_map/all_to_all | solution.py:105
  249.7 0.2 fusion.14
  250.0 1.6 add_convert_fusion
  (54 shorter events, 0.9 us)
Async XLA Ops:
  7.2 98.0 %copy-start = (bf16[4,256,256]{2,1,0:T(8,128)(2,1)S(1)}, bf16[4,256,256]{2,1,0:T(8,128)(2,1)}, u32[]{:S(2)}) copy-start(bf16[4,256,256]{2,1,0:T(8,128)(2,1)} %param.24) | copy-start | bytes 1572868
  7.2 96.9 %reduce-scatter.3.cloned.1.call-start = ((), (), s32[]{:S(2)}) async-start(), calls=%async_computation.5 | async-start | bytes 2359296 | tf_op jit(solution)/shard_map/reduce_scatter | solution.py:54
  32.1 4.3 %copy-start.3 = (bf16[64,3,1024]{2,0,1:T(8,128)(2,1)S(1)}, bf16[64,3,1024]{2,0,1:T(8,128)(2,1)}, u32[]{:S(2)}) copy-start(bf16[64,3,1024]{2,0,1:T(8,128)(2,1)} %param.19) | copy-start | bytes 1179652
  32.1 4.4 %copy-start.8 = (f32[1024]{0:T(1024)S(1)}, f32[1024]{0:T(1024)}, u32[]{:S(2)}) copy-start(f32[1024]{0:T(1024)} %param.26) | copy-start | bytes 12292
  32.1 4.4 %copy-start.6 = (bf16[4,1024]{1,0:T(4,128)(2,1)S(1)}, bf16[4,1024]{1,0:T(4,128)(2,1)}, u32[]{:S(2)}) copy-start(bf16[4,1024]{1,0:T(4,128)(2,1)} %param.23) | copy-start | bytes 24580
  36.3 69.2 %copy-start.14 = (bf16[4,256,256]{2,1,0:T(8,128)(2,1)S(1)}, bf16[4,256,256]{2,1,0:T(8,128)(2,1)}, u32[]{:S(2)}) copy-start(bf16[4,256,256]{2,1,0:T(8,128)(2,1)} %param.25) | copy-start | bytes 1572868
  36.3 69.4 %copy-start.5 = (f32[64,1024]{1,0:T(8,128)S(1)}, f32[64,1024]{1,0:T(8,128)}, u32[]{:S(2)}) copy-start(f32[64,1024]{1,0:T(8,128)} %param.18) | copy-start | bytes 786436
  36.3 97.4 %all-gather.3.cloned.1.call-start = ((), (), s32[]{:S(2)}) async-start(), calls=%async_computation.7 | async-start | bytes 2621440 | tf_op jit(solution)/shard_map/all_gather | solution.py:81
  104.1 1.9 copy-start.4
  106.0 5.9 %copy-start.2 = (f32[64,1024]{1,0:T(8,128)}, f32[64,1024]{1,0:T(8,128)S(1)}, u32[]{:S(2)}) copy-start(f32[64,1024]{1,0:T(8,128)S(1)} %multiply_add_fusion) | copy-start | bytes 786436
  106.0 6.0 %copy-start.7 = (bf16[4096]{0:T(1024)(128)(2,1)S(1)}, bf16[4096]{0:T(1024)(128)(2,1)}, u32[]{:S(2)}) copy-start(bf16[4096]{0:T(1024)(128)(2,1)} %param.28) | copy-start | bytes 24580
  106.0 6.0 %copy-start.10 = (s32[64,2]{0,1:T(2,128)S(1)}, s32[64,2]{0,1:T(2,128)}, u32[]{:S(2)}) copy-start(s32[64,2]{0,1:T(2,128)} %param.32) | copy-start | bytes 1540
  106.0 29.7 %copy-start.1 = (bf16[64,4096]{1,0:T(8,128)(2,1)S(1)}, bf16[64,4096]{1,0:T(8,128)(2,1)}, u32[]{:S(2)}) copy-start(bf16[64,4096]{1,0:T(8,128)(2,1)} %param.17) | copy-start | bytes 1572868
  112.0 117.9 %reduce-scatter.5.cloned.1.call-start = ((), (), s32[]{:S(2)}) async-start(), calls=%async_computation.6 | async-start | bytes 2621440 | tf_op jit(solution)/shard_map/reduce_scatter | solution.py:102
  138.7 54.7 %copy-start.11 = (bf16[1,4096,512]{2,1,0:T(8,128)(2,1)S(1)}, bf16[1,4096,512]{2,1,0:T(8,128)(2,1)}, u32[]{:S(2)}) copy-start(bf16[1,4096,512]{2,1,0:T(8,128)(2,1)} %param.29) | copy-start | bytes 12582916
  193.5 2.2 copy-start.12
  195.7 2.2 copy-start.13
  197.9 37.7 %copy-start.9 = (f32[64,2]{0,1:T(2,128)S(1)}, f32[64,2]{0,1:T(2,128)}, u32[]{:S(2)}) copy-start(f32[64,2]{0,1:T(2,128)} %param.33) | copy-start | bytes 1540
  197.9 37.8 %slice-start = ((bf16[64,3,1024]{2,0,1:T(8,128)(2,1)}), bf16[64,2,1024]{2,0,1:T(8,128)(2,1)S(1)}, s32[]{:S(2)}) async-start(bf16[64,3,1024]{2,0,1:T(8,128)(2,1)} %param.19), calls=%async_computation.8 | async-start | bytes 524288 | tf_op jit(solution)/shard_map/slice | solution.py:63
  229.9 19.8 %all-to-all-start.2 = ((bf16[8,32,1024]{2,1,0:T(8,128)(2,1)}), bf16[8,32,1024]{2,1,0:T(8,128)(2,1)S(1)}, u32[]{:S(2)}, u32[]{:S(2)}) async-start(bf16[8,32,1024]{2,1,0:T(8,128)(2,1)} %reduce-scatter.5.cloned.1.call-done), calls=%async_computation.4 | async-start | bytes 1048576 | tf_op jit(solution)/shard_map/all_to_all | solution.py:105
Sparse Core Ops, SparseCore 0:
  36.5 67.5 reduce-scatter.2
  112.1 21.6 all-gather.2
  200.6 29.2 reduce-scatter.4
